TPU v7x, 128 devices: a whole 4x4x4 slice. The times are simulated.
128 devices in a mesh: st: 64 (over z, y, x), tp: 2 (over core).
Axes of the slice: x: 4, y: 4, z: 4, core: 2. Of those that a mesh axis runs over, the one named last changes fastest.
Arguments:
- tokens: bfloat16 [65536, 2048], P('st', 'tp'), may hold values from -6 to 6
- passage_ids: int32 [1024, 2], P('st'), may hold values from 0 to 1023, as said below
- passage_store: bfloat16 [1024, 64, 2048], P('st'), may hold values from -6 to 6
- norm_gain: bfloat16 [2048], replicated, may hold values from 0.099609375 to 1.8984375
- conv_value_weight: bfloat16 [2048, 1536], P(None, 'tp'), may hold values from -0.125 to 0.125
- conv_gate_weight: bfloat16 [2048, 1536], P(None, 'tp'), may hold values from -0.125 to 0.125
- conv_weight: bfloat16 [31, 1536], P(None, 'tp'), may hold values from -1 to 1
- ln_gain: bfloat16 [1536], P('tp'), may hold values from 0.099609375 to 1.8984375
- query_weight: bfloat16 [2048, 512], P(None, 'tp'), may hold values from -0.125 to 0.125
- query_gain: bfloat16 [512], P('tp'), may hold values from 0.5 to 10
- passage_gain: bfloat16 [2048], replicated, may hold values from 0.099609375 to 1.8984375
- key_weight: bfloat16 [2048, 512], P(None, 'tp'), may hold values from -0.125 to 0.125
- value_weight: bfloat16 [2048, 512], P(None, 'tp'), may hold values from -0.125 to 0.125
- key_gain: bfloat16 [512], P('tp'), may hold values from 0.5 to 10
- memory_gate: bfloat16 [512], P('tp'), may hold values from 0.29882812 to 1.5
- conv_out_weight: bfloat16 [1536, 2048], P('tp'), may hold values from -0.125 to 0.125
- memory_out_weight: bfloat16 [512, 2048], P('tp'), may hold values from -0.125 to 0.125
Outputs:
- layer_out: bfloat16 [65536, 2048], P(('st', 'tp'))
Inputs may be any that keep to these rules, and one draw needn't show every extreme that they name: The owner of passage p is p // 16. Among the 32 entries of the rows of passage_ids that lie on one index of st (aligned runs of 16 rows, that is the blocks of one index of st), no owner is named more than 1 times, and in every such run some owner is named exactly 1 times.
All inputs are finite; a program needn't handle non-finite values.
Results may differ from a plain program's by a relative error of at most 0.008.
The roundings to bfloat16 on the way count: a program that leaves them out, or rounds other values in their place, can miss the bound.
Values may be sent and summed in bfloat16 or wider, within the bound.
No kernel may reach another device: no remote copies, remote signals or barrier semaphores. Data moves between devices by JAX's collectives and lax.ppermute only.
A program may use at most 192 MiB of HBM per device.

v0:
```python
import jax
import jax.numpy as jnp
from jax import lax
from jax.experimental import pallas as pl
from jax.experimental.pallas import tpu as pltpu
from jax.sharding import PartitionSpec as P

D = 2048
HALF_D = 1024
C_A = 1536
C_DEV = 768
MEM_HD = 64
MEM_DEV = 256
KW = 31
SEQ_LEN = 512
BLOCK = 64
PLEN = 64
PASS_DEV = 16
OWNER_SHIFT = 4
NORM_EPS = 1e-06
LAYER_EPS = 1e-05

KV_TILE = 512
TOK_TILE = 256
OUT_TILE = 256
OUT_COLS = 512
ATT_TILE = 256
ATT_GROUP = 8
LANES = 128
CONV_ROWS = 128
NORM_ROWS = 16
HISTORY = 32

F32 = jnp.float32
BF16 = jnp.bfloat16


def matmul(a, b):
    return lax.dot_general(a, b, (((1,), (0,)), ((), ())), preferred_element_type=F32)


def matmul_t(a, b):
    return lax.dot_general(a, b, (((1,), (1,)), ((), ())), preferred_element_type=F32)


def row_norm(rows, gain):
    widened = rows.astype(F32)
    factor = lax.rsqrt(jnp.sum(widened * widened, axis=1, keepdims=True) * (1.0 / D) + NORM_EPS)
    return (widened * factor * gain).astype(BF16)


def head_norm(product, gain):
    width = product.shape[1]
    rows = lax.broadcasted_iota(jnp.int32, (width, width), 0) // MEM_HD
    cols = lax.broadcasted_iota(jnp.int32, (width, width), 1) // MEM_HD
    same_head = jnp.where(rows == cols, 1.0, 0.0).astype(BF16)
    squares = product * product
    coarse = squares.astype(BF16)
    fine = (squares - coarse.astype(F32)).astype(BF16)
    total = matmul(coarse, same_head) + matmul(fine, same_head)
    return product * lax.rsqrt(total * (1.0 / MEM_HD) + NORM_EPS) * gain


def wide_row(ref):
    values = ref[...].astype(F32)
    return jnp.concatenate([values[i : i + 1, :] for i in range(values.shape[0])], axis=1)


def kv_kernel(
    rows_hbm, gain_hbm, wk_hbm, wv_hbm, kg_hbm, out_ref,
    rows_ref, gain_ref, w_ref, kg_ref, even, odd, r_sem, w_sem
):
    chunks = rows_hbm.shape[0] // KV_TILE
    span = lambda c: pl.ds(c * KV_TILE, KV_TILE)
    row_copies = [pltpu.make_async_copy(rows_hbm.at[span(c)], rows_ref.at[span(c)], r_sem.at[c]) for c in range(chunks)]
    wk_copy = pltpu.make_async_copy(wk_hbm, w_ref.at[:, :MEM_DEV], w_sem.at[0])
    wv_copy = pltpu.make_async_copy(wv_hbm, w_ref.at[:, MEM_DEV:], w_sem.at[1])
    gain_copy = pltpu.make_async_copy(gain_hbm, gain_ref, w_sem.at[2])
    kg_copy = pltpu.make_async_copy(kg_hbm, kg_ref, w_sem.at[3])
    for c in [gain_copy, kg_copy, row_copies[0], wk_copy, wv_copy, *row_copies[1:]]:
        c.start()
    gain_copy.wait()
    kg_copy.wait()
    gain = wide_row(gain_ref)
    key_gain = wide_row(kg_ref)
    held = (even, odd)

    def normalise(c):
        for r in range(0, KV_TILE, NORM_ROWS):
            rows = rows_ref[c * KV_TILE + r : c * KV_TILE + r + NORM_ROWS, :]
            held[c % 2][r : r + NORM_ROWS, :] = row_norm(rows, gain)

    row_copies[0].wait()
    normalise(0)
    wk_copy.wait()
    wv_copy.wait()
    for c in range(chunks):
        if c + 1 < chunks:
            row_copies[c + 1].wait()
            normalise(c + 1)
        both = matmul(held[c % 2][...], w_ref[...])
        out_ref[span(c), :MEM_DEV] = head_norm(both[:, :MEM_DEV], key_gain).astype(BF16)
        out_ref[span(c), MEM_DEV:] = both[:, MEM_DEV:].astype(BF16)


def resident(shape):
    zeros = (0,) * len(shape)
    return pl.BlockSpec(shape, lambda *_: zeros, pipeline_mode=pl.Buffered(1))


HBM = pl.BlockSpec(memory_space=pl.ANY)
ONCHIP = pl.BlockSpec(memory_space=pltpu.VMEM)


def onchip(*arrays):
    return tuple(pltpu.with_memory_space_constraint(a, pltpu.VMEM) for a in arrays)


def offchip(*arrays):
    return tuple(pltpu.with_memory_space_constraint(a, pltpu.HBM) for a in arrays)


def grant(mib):
    return pltpu.CompilerParams(vmem_limit_bytes=mib << 20)


def project_store(rows, passage_gain, key_weight, value_weight, key_gain):
    n = rows.shape[0]
    return pl.pallas_call(
        kv_kernel,
        out_shape=pltpu.VMEM((n, 2 * MEM_DEV), BF16),
        in_specs=[HBM] * 5,
        out_specs=ONCHIP,
        scratch_shapes=[
            pltpu.VMEM((n, D), BF16),
            pltpu.VMEM((D // LANES, LANES), BF16),
            pltpu.VMEM((D, 2 * MEM_DEV), BF16),
            pltpu.VMEM((MEM_DEV // LANES, LANES), BF16),
            pltpu.VMEM((KV_TILE, D), BF16),
            pltpu.VMEM((KV_TILE, D), BF16),
            pltpu.SemaphoreType.DMA((n // KV_TILE,)),
            pltpu.SemaphoreType.DMA((4,)),
        ],
        compiler_params=grant(24),
        cost_estimate=pl.CostEstimate(flops=2 * n * D * 2 * MEM_DEV, transcendentals=0, bytes_accessed=8 << 20),
        name="project_store",
    )(*offchip(rows, passage_gain, key_weight, value_weight, key_gain))


def slots_kernel(ids_ref, kv_ref, out_hbm, row_ref, sem):
    count = out_hbm.shape[0]
    local = ids_ref[...] ^ (lax.axis_index("st") * PASS_DEV)
    asked = jnp.where(local < PASS_DEV, local, 0)
    asked = jnp.sum(asked[:, 0, :] + asked[:, 1, :], axis=1, keepdims=True).astype(F32)
    square = jnp.concatenate([jnp.broadcast_to(asked, (count, LANES)), jnp.zeros((LANES - count, LANES), F32)], axis=0)
    row_ref[...] = square.T[:8, :].astype(jnp.int32)
    copies = [pltpu.make_async_copy(kv_ref.at[row_ref[0, s]], out_hbm.at[s], sem.at[s]) for s in range(count)]
    for c in copies:
        c.start()
    for c in copies:
        c.wait()


def fill_slots(ids, kv):
    count = ids.shape[0]
    return pl.pallas_call(
        slots_kernel,
        out_shape=pltpu.HBM((count, PLEN, 2 * MEM_DEV), BF16),
        in_specs=[ONCHIP, ONCHIP],
        out_specs=HBM,
        scratch_shapes=[
            pltpu.VMEM((8, LANES), jnp.int32),
            pltpu.SemaphoreType.DMA((count,)),
        ],
        compiler_params=grant(2),
        name="fill_slots",
    )(*onchip(ids, kv))


def token_kernel(
    tp_ref, own_ref, peer_ref, gain_ref, wv_ref, wg_ref, wq_ref, cw_ref, qg_ref, filt_ref, stat_ref, q_ref, xs_ref, taps_ref,
    own_n, peer_n
):
    tile = pl.program_id(0)
    me = tp_ref[0]
    own_at = pl.multiple_of(me * HALF_D, HALF_D)
    peer_at = pl.multiple_of((1 - me) * HALF_D, HALF_D)
    own_gain = wide_row(gain_ref.at[me])
    peer_gain = wide_row(gain_ref.at[1 - me])
    for r in range(0, TOK_TILE, NORM_ROWS):
        rows = slice(r, r + NORM_ROWS)
        own = own_ref[rows, :].astype(F32)
        peer = peer_ref[rows, :].astype(F32)
        total = jnp.sum(own * own + peer * peer, axis=1, keepdims=True)
        factor = lax.rsqrt(total * (1.0 / D) + NORM_EPS)
        own_n[rows, :] = (own * factor * own_gain).astype(BF16)
        peer_n[rows, :] = (peer * factor * peer_gain).astype(BF16)

    def product(w_ref):
        own_part = matmul(own_n[...], w_ref[pl.ds(own_at, HALF_D), :])
        return own_part + matmul(peer_n[...], w_ref[pl.ds(peer_at, HALF_D), :])

    q_ref[...] = head_norm(product(wq_ref), wide_row(qg_ref) * MEM_HD ** (-0.5)).astype(BF16)
    gated = (product(wv_ref) * jax.nn.sigmoid(product(wg_ref))).astype(BF16)

    @pl.when(tile % (SEQ_LEN // TOK_TILE) == 0)
    def _():
        xs_ref[:HISTORY, :] = jnp.zeros((HISTORY, C_DEV), F32)

    taps_ref[...] = cw_ref[...].astype(F32)
    xs_ref[HISTORY:, :] = gated.astype(F32)
    first = HISTORY - (KW - 1)
    for base in range(0, TOK_TILE, CONV_ROWS):
        sums = jnp.zeros((CONV_ROWS, LANES), F32)
        squares = jnp.zeros((CONV_ROWS, LANES), F32)
        for lane in range(0, C_DEV, LANES):
            lanes = slice(lane, lane + LANES)
            acc = None
            for r in range(8):
                steps = [s for s in range(first, first + KW) if s % 8 == r]
                reach = max(steps) - r + CONV_ROWS
                shifted = xs_ref[base + r : base + r + reach, lanes]
                part = None
                for s in steps:
                    term = shifted[s - r : s - r + CONV_ROWS] * taps_ref[s - first : s - first + 1, lanes]
                    part = term if part is None else part + term
                acc = part if acc is None else acc + part
            filt_ref[base : base + CONV_ROWS, lanes] = acc
            sums = sums + acc
            squares = squares + acc * acc
        stat_ref[base : base + CONV_ROWS, 0:1] = jnp.sum(sums, axis=1, keepdims=True)
        stat_ref[base : base + CONV_ROWS, 1:2] = jnp.sum(squares, axis=1, keepdims=True)
    xs_ref[:HISTORY, :] = xs_ref[TOK_TILE:, :]


def token_branch(me, own, peer, gain, wv, wg, wq, cw, qg):
    n = own.shape[0]
    tile = lambda width: pl.BlockSpec((TOK_TILE, width), lambda i, s: (i, 0))
    return pl.pallas_call(
        token_kernel,
        out_shape=(
            jax.ShapeDtypeStruct((n, C_DEV), F32),
            jax.ShapeDtypeStruct((n, 2), F32),
            jax.ShapeDtypeStruct((n, MEM_DEV), BF16),
        ),
        grid_spec=pltpu.PrefetchScalarGridSpec(
            num_scalar_prefetch=1,
            grid=(n // TOK_TILE,),
            in_specs=[
                tile(HALF_D),
                tile(HALF_D),
                resident((2, HALF_D // LANES, LANES)),
                resident((D, C_DEV)),
                resident((D, C_DEV)),
                resident((D, MEM_DEV)),
                resident((KW, C_DEV)),
                resident((MEM_DEV // LANES, LANES)),
            ],
            out_specs=(tile(C_DEV), tile(2), tile(MEM_DEV)),
            scratch_shapes=[
                pltpu.VMEM((HISTORY + TOK_TILE, C_DEV), F32),
                pltpu.VMEM((KW, C_DEV), F32),
                pltpu.VMEM((TOK_TILE, HALF_D), BF16),
                pltpu.VMEM((TOK_TILE, HALF_D), BF16),
            ],
        ),
        cost_estimate=pl.CostEstimate(flops=20 * n * D * 768, transcendentals=0, bytes_accessed=16 << 20),
        name="token_branch",
    )(me, own, peer, gain, wv, wg, wq, cw, qg)


def swish_kernel(filt_ref, own_ref, peer_ref, gain_ref, out_ref):
    stats = (own_ref[...] + peer_ref[...]) * (1.0 / C_A)
    mean = stats[:, 0:1]
    var = stats[:, 1:2] - mean * mean
    scaled = (filt_ref[...] - mean) * lax.rsqrt(var + LAYER_EPS) * wide_row(gain_ref)
    out_ref[...] = (scaled * jax.nn.sigmoid(scaled)).astype(BF16)


def channel_swish(half, filtered, own_stats, peer_stats, gain):
    n = filtered.shape[0] // 2
    steps = n // OUT_TILE
    tile = lambda width: pl.BlockSpec((OUT_TILE, width), lambda i, h: (h[0] * steps + i, 0))
    return pl.pallas_call(
        lambda half_ref, *refs: swish_kernel(*refs),
        out_shape=jax.ShapeDtypeStruct((n, C_DEV), BF16),
        grid_spec=pltpu.PrefetchScalarGridSpec(
            num_scalar_prefetch=1,
            grid=(steps,),
            in_specs=[tile(C_DEV), tile(2), tile(2), resident((C_DEV // LANES, LANES))],
            out_specs=pl.BlockSpec((OUT_TILE, C_DEV), lambda i, h: (i, 0)),
        ),
        cost_estimate=pl.CostEstimate(flops=n * D * 768, transcendentals=0, bytes_accessed=4 << 20),
        name="channel_swish",
    )(half, filtered, own_stats, peer_stats, gain)


def pair_kernel(own_ref, peer_ref, w_own_hbm, w_peer_hbm, out_ref, w_own_ref, w_peer_ref, sem):
    parts = D // OUT_COLS
    cols = lambda c: pl.ds(c * OUT_COLS, OUT_COLS)
    copies = [
        pltpu.make_async_copy(hbm.at[:, cols(c)], ref.at[:, cols(c)], sem.at[i, c])
        for c in range(parts)
        for i, (hbm, ref) in enumerate(((w_own_hbm, w_own_ref), (w_peer_hbm, w_peer_ref)))
    ]
    for c in copies:
        c.start()
    for c in range(parts):
        copies[2 * c].wait()
        copies[2 * c + 1].wait()
        own_part = matmul(own_ref[...], w_own_ref[:, cols(c)])
        out_ref[:, cols(c)] = (own_part + matmul(peer_ref[...], w_peer_ref[:, cols(c)])).astype(BF16)


def conv_product(own, peer, w_own, w_peer):
    n = own.shape[0]
    return pl.pallas_call(
        pair_kernel,
        out_shape=pltpu.HBM((n, D), BF16),
        in_specs=[ONCHIP, ONCHIP, HBM, HBM],
        out_specs=pl.BlockSpec((n, D), lambda: (0, 0)),
        scratch_shapes=[
            pltpu.VMEM((C_DEV, D), BF16),
            pltpu.VMEM((C_DEV, D), BF16),
            pltpu.SemaphoreType.DMA((2, D // OUT_COLS)),
        ],
        compiler_params=grant(16),
        cost_estimate=pl.CostEstimate(flops=4 * n * D * C_DEV, transcendentals=0, bytes_accessed=12 << 20),
        name="conv_product",
    )(*onchip(own, peer), *offchip(w_own, w_peer))


def attend_blocks(blocks, kv_ref, q_ref, base, gate):
    heads = MEM_DEV // MEM_HD
    lane_head = lax.broadcasted_iota(jnp.int32, (BLOCK, MEM_DEV), 1) // MEM_HD
    scores = []
    for b in blocks:
        q = q_ref[pl.ds(base + b * BLOCK, BLOCK), :]
        spread = jnp.concatenate([jnp.where(lane_head == h, q, jnp.zeros_like(q)) for h in range(heads)], axis=0)
        scores.append(matmul_t(spread, kv_ref[2 * b : 2 * b + 2, :, :MEM_DEV].reshape(2 * PLEN, MEM_DEV)))
    expanded = [jnp.exp(s - jnp.max(s, axis=1, keepdims=True)) for s in scores]
    weights = [(e * (1.0 / jnp.sum(e, axis=1, keepdims=True))).astype(BF16) for e in expanded]
    rows = []
    for w, b in zip(weights, blocks):
        mixed = matmul(w, kv_ref[2 * b : 2 * b + 2, :, MEM_DEV:].reshape(2 * PLEN, MEM_DEV))
        attended = mixed[:BLOCK]
        for h in range(1, heads):
            attended = jnp.where(lane_head == h, mixed[h * BLOCK : (h + 1) * BLOCK], attended)
        rows.append((attended * gate).astype(BF16))
    return jnp.concatenate(rows, axis=0)


def attend_all(out_ref, kv_ref, q_ref, base, gate, arrived):
    size = ATT_GROUP * BLOCK
    for g in range(out_ref.shape[0] // size):
        arrived(g)
        blocks = range(g * ATT_GROUP, (g + 1) * ATT_GROUP)
        out_ref[pl.ds(g * size, size), :] = attend_blocks(blocks, kv_ref, q_ref, base, gate)


def attend_kernel(
    owner_ref, recv_hbm, q_ref, gate_ref, out_ref, next_kv_ref, next_q_ref, kv_ref, sem, next_sem, q_sem
):
    count = kv_ref.shape[0]
    n = next_q_ref.shape[0]
    second = lax.axis_index("tp")
    first = 1 - second
    low, high = ([owner_ref[0, h * count + i] for i in range(count)] for h in range(2))
    owners = [jnp.where(first == 0, a, b) for a, b in zip(low, high)]
    others = [jnp.where(first == 0, b, a) for a, b in zip(low, high)]
    copies = [pltpu.make_async_copy(recv_hbm.at[owners[i]], kv_ref.at[i], sem.at[i]) for i in range(count)]
    later = [
        pltpu.make_async_copy(recv_hbm.at[others[i]], next_kv_ref.at[i], next_sem.at[i])
        for i in range(count)
    ] + [pltpu.make_async_copy(q_ref.at[pl.ds(pl.multiple_of(second * n, n), n), :], next_q_ref, q_sem)]
    for c in copies:
        c.start()
    gate = jnp.tanh(wide_row(gate_ref))

    def arrived(g):
        for c in copies[2 * g * ATT_GROUP : 2 * (g + 1) * ATT_GROUP]:
            c.wait()
        if g == 0:
            for c in later:
                c.start()

    attend_all(out_ref, kv_ref, q_ref, pl.multiple_of(first * n, n), gate, arrived)
    for c in later:
        c.wait()


def attend_first(owners, received, queries, gate):
    n = queries.shape[0] // 2
    count = owners.shape[1] // 2
    return pl.pallas_call(
        attend_kernel,
        out_shape=(
            pltpu.VMEM((n, MEM_DEV), BF16),
            pltpu.VMEM((count, PLEN, 2 * MEM_DEV), BF16),
            pltpu.VMEM((n, MEM_DEV), BF16),
        ),
        in_specs=[ONCHIP, HBM, ONCHIP, ONCHIP],
        out_specs=(ONCHIP, ONCHIP, ONCHIP),
        scratch_shapes=[
            pltpu.VMEM((count, PLEN, 2 * MEM_DEV), BF16),
            pltpu.SemaphoreType.DMA((count,)),
            pltpu.SemaphoreType.DMA((count,)),
            pltpu.SemaphoreType.DMA(()),
        ],
        compiler_params=grant(8),
        cost_estimate=pl.CostEstimate(flops=n * D * 256, transcendentals=0, bytes_accessed=2 << 20),
        name="attend_first",
    )(*onchip(owners), *offchip(received), *onchip(queries, gate))


def attend_rest_kernel(kv_ref, q_ref, gate_ref, out_ref):
    attend_all(out_ref, kv_ref, q_ref, 0, jnp.tanh(wide_row(gate_ref)), lambda g: None)


def attend_rest(kv, queries, gate):
    n = queries.shape[0]
    return pl.pallas_call(
        attend_rest_kernel,
        out_shape=pltpu.VMEM((n, MEM_DEV), BF16),
        in_specs=[ONCHIP] * 3,
        out_specs=ONCHIP,
        compiler_params=grant(6),
        cost_estimate=pl.CostEstimate(flops=n * D * 256, transcendentals=0, bytes_accessed=2 << 20),
        name="attend_rest",
    )(*onchip(kv, queries, gate))


def finish_kernel(own_ref, peer_ref, w_own_ref, w_peer_ref, conv_ref, out_hbm, out_ref, out_sem):
    groups = out_ref.shape[0] // ATT_TILE
    span = lambda g: pl.ds(g * ATT_TILE, ATT_TILE)
    out_copies = [pltpu.make_async_copy(out_ref.at[span(g)], out_hbm.at[span(g)], out_sem.at[g]) for g in range(groups)]
    for g in range(groups):
        memory = matmul(own_ref[span(g), :], w_own_ref[...]) + matmul(peer_ref[span(g), :], w_peer_ref[...])
        out_ref[span(g), :] = (conv_ref[span(g), :].astype(F32) + memory).astype(BF16)
        out_copies[g].start()
    for c in out_copies:
        c.wait()


def finish(own, peer, w_own, w_peer, conv_sum):
    n = conv_sum.shape[0]
    return pl.pallas_call(
        finish_kernel,
        out_shape=pltpu.HBM((n, D), BF16),
        in_specs=[ONCHIP] * 5,
        out_specs=HBM,
        scratch_shapes=[pltpu.VMEM((n, D), BF16), pltpu.SemaphoreType.DMA((n // ATT_TILE,))],
        compiler_params=grant(12),
        cost_estimate=pl.CostEstimate(flops=4 * n * D * MEM_DEV, transcendentals=0, bytes_accessed=8 << 20),
        name="finish",
    )(*onchip(own, peer, w_own, w_peer, conv_sum))


def body(
    tokens,
    passage_ids,
    passage_store,
    norm_gain,
    conv_value_weight,
    conv_gate_weight,
    conv_weight,
    ln_gain,
    query_weight,
    query_gain,
    passage_gain,
    key_weight,
    value_weight,
    key_gain,
    memory_gate,
    conv_out_weight,
    memory_out_weight,
):
    owner_count = lax.axis_size("st")
    swap = [(0, 1), (1, 0)]
    me = lax.axis_index("tp").astype(jnp.int32).reshape(1)

    ids = lax.all_to_all(jnp.broadcast_to(passage_ids.T, (owner_count, *passage_ids.shape[::-1])), "st", 0, 0, tiled=True)
    peer_tokens = lax.ppermute(tokens, "tp", swap)
    peer_conv_weight = lax.ppermute(conv_out_weight, "tp", swap)
    peer_memory_weight = lax.ppermute(memory_out_weight, "tp", swap)

    kv = project_store(
        passage_store.reshape(-1, D),
        passage_gain.reshape(-1, LANES),
        key_weight,
        value_weight,
        key_gain.reshape(-1, LANES),
    ).reshape(PASS_DEV, PLEN, 2 * MEM_DEV)
    sent = fill_slots(ids, kv)
    received = lax.all_to_all(sent, "st", 0, 0, tiled=True)

    filtered, own_stats, queries = token_branch(
        me,
        tokens,
        peer_tokens,
        norm_gain.reshape(2, -1, LANES),
        conv_value_weight,
        conv_gate_weight,
        query_weight,
        conv_weight,
        query_gain.reshape(-1, LANES),
    )
    peer_stats = lax.ppermute(own_stats, "tp", swap)
    conv_theirs = channel_swish(1 - me, filtered, own_stats, peer_stats, ln_gain.reshape(-1, LANES))
    conv_peer = lax.ppermute(conv_theirs, "tp", swap)
    conv_mine = channel_swish(me, filtered, own_stats, peer_stats, ln_gain.reshape(-1, LANES))
    conv_sum = conv_product(conv_mine, conv_peer, conv_out_weight, peer_conv_weight)

    owners = lax.optimization_barrier((passage_ids, filtered))[0].reshape(1, -1) >> OWNER_SHIFT
    gate = memory_gate.reshape(-1, LANES)
    memory_theirs, next_kv, next_queries = attend_first(owners, received, queries, gate)
    memory_peer = lax.ppermute(memory_theirs, "tp", swap)
    memory_mine = attend_rest(next_kv, next_queries, gate)
    return finish(memory_mine, memory_peer, memory_out_weight, peer_memory_weight, conv_sum)


def solution(mesh):
    return jax.shard_map(
        body,
        mesh=mesh,
        in_specs=(
            P("st", "tp"),
            P("st", None),
            P("st", None, None),
            P(),
            P(None, "tp"),
            P(None, "tp"),
            P(None, "tp"),
            P("tp"),
            P(None, "tp"),
            P("tp"),
            P(),
            P(None, "tp"),
            P(None, "tp"),
            P("tp"),
            P("tp"),
            P("tp", None),
            P("tp", None),
        ),
        out_specs=P(("st", "tp"), None),
        check_vma=False,
    )
```

profile of v0, /device:TPU:1, one launch (start us, length us, event | category | flops | bytes accessed | tf_op | source)
XLA Modules:
  0.0 104.6 jit_solution(11564621260991605868)
XLA Ops:
  0.0 1.4 %collective-permute-start = (bf16[1024,1024]{1,0:T(8,128)(2,1)}, bf16[1024,1024]{1,0:T(8,128)(2,1)}, u32[]{:S(2)}, u32[]{:S(2)}) collective-permute-start(bf16[1024,1024]{1,0:T(8,128)(2,1)} %own_ref.1), channel_id=1, source_target_pairs={{0,1},{1,0},{2,3},{3,2},{4,5},{5,4},{6,7},{7,6},{8,9},{9,8},{10,11... | collective-permute-start | bytes 6291464 | tf_op jit(solution)/shard_map/ppermute | solution.py:483
  1.4 1.3 %broadcast_in_dim.3 = s32[64,2,16]{2,1,0:T(2,128)} broadcast(s32[2,16]{1,0:T(2,128)} %bitcast.15), dimensions={1,2} | broadcast | bytes 8320 | tf_op jit(solution)/shard_map/broadcast_in_dim | solution.py:482
  2.7 11.2 %all-to-all-start = ((s32[64,2,16]{2,1,0:T(2,128)}), s32[64,2,16]{2,1,0:T(2,128)S(1)}, u32[]{:S(2)}, u32[]{:S(2)}) async-start(s32[64,2,16]{2,1,0:T(2,128)} %broadcast_in_dim.3), calls=%async_computation | async-start | bytes 131072 | tf_op jit(solution)/shard_map/all_to_all | solution.py:482
  14.0 5.9 %project_store.1 = bf16[1024,512]{1,0:T(8,128)(2,1)S(1)} custom-call(bf16[1024,2048]{1,0:T(8,128)(2,1)} %bitcast.16, bf16[16,128]{1,0:T(8,128)(2,1)} %bitcast.17, bf16[2048,256]{1,0:T(8,128)(2,1)} %wk_hbm.1, bf16[2048,256]{1,0:T(8,128)(2,1)} %wv_hbm.1, bf16[2,128]{1,0:T(2,128)(2,1)} %bitcast.19), custom_call_target="tpu_custom_call" | custom-call | flops 2147483648 | bytes 8388608 | tf_op jit(solution)/shard_map/project_store/pallas_call | solution.py:129
  19.8 2.6 %all-to-all-done.ids_ref = s32[64,2,16]{2,1,0:T(2,128)S(1)} async-done(((s32[64,2,16]{2,1,0:T(2,128)}), s32[64,2,16]{2,1,0:T(2,128)S(1)}, u32[]{:S(2)}, u32[]{:S(2)}) %all-to-all-start) | async-done | bytes 8224 | tf_op jit(solution)/shard_map/all_to_all | solution.py:482
  22.4 2.9 %fill_slots.1 = bf16[64,64,512]{2,1,0:T(8,128)(2,1)} custom-call(s32[64,2,16]{2,1,0:T(2,128)S(1)} %all-to-all-done.ids_ref, bf16[16,64,512]{2,1,0:T(8,128)(2,1)S(1)} %bitcast.10), custom_call_target="tpu_custom_call" | custom-call | tf_op jit(solution)/shard_map/fill_slots/pallas_call | solution.py:166
  25.3 7.5 %all-to-all-start.1 = ((bf16[64,64,512]{2,1,0:T(8,128)(2,1)}), bf16[64,64,512]{2,1,0:T(8,128)(2,1)}, u32[]{:S(2)}, u32[]{:S(2)}) async-start(bf16[64,64,512]{2,1,0:T(8,128)(2,1)} %fill_slots.1), calls=%async_computation.1 | async-start | bytes 8388608 | tf_op jit(solution)/shard_map/all_to_all | solution.py:495
  32.8 0.9 collective-permute-start.5
  33.7 0.0 collective-permute-done.peer_ref
  33.7 24.8 %token_branch.1 = (f32[1024,768]{1,0:T(8,128)}, f32[1024,2]{1,0:T(8,128)}, bf16[1024,256]{1,0:T(8,128)(2,1)}) custom-call(s32[1]{0:T(128)} %bitcast.tp_ref.half_ref, bf16[1024,1024]{1,0:T(8,128)(2,1)} %own_ref.1, bf16[1024,1024]{1,0:T(8,128)(2,1)} %collective-permute-done.peer_ref, bf16[2,8,128]{2,1,0:T(8,128)(2,1)} %bitcast.18, bf16[2048,768]{1,0:T(8,128)(2,1)} %wv_ref.1, ...), custom_call_target="tpu_custom_call" | custom-call | flops 32212254720 | bytes 16777216 | tf_op jit(solution)/shard_map/token_branch/pallas_call | solution.py:239
  58.6 0.0 copy-start.1
  58.6 0.0 copy-start.6
  58.6 0.1 collective-permute-start.3
  58.7 2.1 %collective-permute-done.3.refs_2_ = f32[1024,2]{1,0:T(8,128)S(1)} collective-permute-done((f32[1024,2]{1,0:T(8,128)}, f32[1024,2]{1,0:T(8,128)S(1)}, u32[]{:S(2)}, u32[]{:S(2)}) %collective-permute-start.3) | collective-permute-done | bytes 8224 | tf_op jit(solution)/shard_map/ppermute | solution.py:508
  60.8 0.0 copy-start.5
  60.8 0.8 copy-done.5
  61.6 2.7 %channel_swish.3 = bf16[512,768]{1,0:T(8,128)(2,1)} custom-call(s32[1]{0:T(128)S(6)} %sub.3.half_ref, f32[1024,768]{1,0:T(8,128)} %get-tuple-element.12.refs_0_, f32[1024,2]{1,0:T(8,128)} %get-tuple-element.18.refs_1_, f32[1024,2]{1,0:T(8,128)} %copy-done.5, bf16[6,128]{1,0:T(8,128)(2,1)} %bitcast.13), custom_call_target="tpu_custom_call" | custom-call | flops 805306368 | bytes 4194304 | tf_op jit(solution)/shard_map/channel_swish/pallas_call | solution.py:284
  64.2 0.0 copy-start.3
  64.2 0.0 copy-start.4
  64.3 0.3 collective-permute-start.4
  64.5 0.0 copy-done.1
  64.5 0.4 collective-permute-start.2
  64.9 0.0 copy-done.6
  64.9 0.1 copy.19
  65.0 0.1 shift_right_arithmetic.10.owner_ref
  65.1 2.7 %channel_swish.2.own_ref = bf16[512,768]{1,0:T(8,128)(2,1)} custom-call(s32[1]{0:T(128)} %bitcast.tp_ref.half_ref, f32[1024,768]{1,0:T(8,128)} %get-tuple-element.12.refs_0_, f32[1024,2]{1,0:T(8,128)} %get-tuple-element.18.refs_1_, f32[1024,2]{1,0:T(8,128)} %copy-done.5, bf16[6,128]{1,0:T(8,128)(2,1)} %bitcast.14), custom_call_target="tpu_custom_call" | custom-call | flops 805306368 | bytes 4194304 | tf_op jit(solution)/shard_map/channel_swish/pallas_call | solution.py:284
  67.8 0.0 copy-start.2
  67.8 19.2 %all-to-all-done.1.recv_hbm = bf16[64,64,512]{2,1,0:T(8,128)(2,1)} async-done(((bf16[64,64,512]{2,1,0:T(8,128)(2,1)}), bf16[64,64,512]{2,1,0:T(8,128)(2,1)}, u32[]{:S(2)}, u32[]{:S(2)}) %all-to-all-start.1) | async-done | bytes 4194336 | tf_op jit(solution)/shard_map/all_to_all | solution.py:495
  87.0 0.0 copy-done.3
  87.0 0.0 copy-done.4
  87.0 2.9 %attend_first.1 = (bf16[512,256]{1,0:T(8,128)(2,1)S(1)}, bf16[16,64,512]{2,1,0:T(8,128)(2,1)S(1)}, bf16[512,256]{1,0:T(8,128)(2,1)S(1)}) custom-call(s32[1,32]{1,0:T(1,128)S(1)} %shift_right_arithmetic.10.owner_ref, bf16[64,64,512]{2,1,0:T(8,128)(2,1)} %all-to-all-done.1.recv_hbm, bf16[1024,256]{1,0:T(8,128)(2,1)S(1)} %copy-done.3, bf16[2,128]{1,0:T(2,128)(2,1)S(1)} %bitcast.11), custom_call_target="tpu_custom_call" | custom-call | flops 268435456 | bytes 2097152 | tf_op jit(solution)/shard_map/attend_first/pallas_call | solution.py:395
  89.9 1.8 %collective-permute-start.1 = (bf16[512,256]{1,0:T(8,128)(2,1)S(1)}, bf16[512,256]{1,0:T(8,128)(2,1)S(1)}, u32[]{:S(2)}, u32[]{:S(2)}) collective-permute-start(bf16[512,256]{1,0:T(8,128)(2,1)S(1)} %get-tuple-element.17), channel_id=1, source_target_pairs={{0,1},{1,0},{2,3},{3,2},{4,5},{5,4},{6,7},{7,6},{8,9},{9,8},{10,11... | collective-permute-start | bytes 786440 | tf_op jit(solution)/shard_map/ppermute | solution.py:517
  91.7 0.0 collective-permute-done.4.peer_ref
  91.7 0.0 collective-permute-done.5.w_peer_hbm
  91.7 0.0 copy-done.2
  91.7 7.8 %conv_product.1.conv_ref = bf16[512,2048]{1,0:T(8,128)(2,1)} custom-call(bf16[512,768]{1,0:T(8,128)(2,1)S(1)} %copy-done.2, bf16[512,768]{1,0:T(8,128)(2,1)} %collective-permute-done.4.peer_ref, bf16[768,2048]{1,0:T(8,128)(2,1)} %w_own_hbm.1, bf16[768,2048]{1,0:T(8,128)(2,1)} %collective-permute-done.5.w_peer_hbm), custom_call_target="tpu_custom_call" | custom-call | flops 3221225472 | bytes 12582912 | tf_op jit(solution)/shard_map/conv_product/pallas_call | solution.py:317
  99.6 1.0 attend_rest.1.own_ref
  100.5 0.0 collective-permute-done.2.w_peer_ref
  100.6 0.0 collective-permute-done.1.peer_ref
  100.6 0.0 copy-start
  100.6 1.6 %copy-done = bf16[512,2048]{1,0:T(8,128)(2,1)S(1)} copy-done((bf16[512,2048]{1,0:T(8,128)(2,1)S(1)}, bf16[512,2048]{1,0:T(8,128)(2,1)}, u32[]{:S(2)}) %copy-start) | copy-done | bytes 2097176
  102.2 2.2 %finish.1 = bf16[512,2048]{1,0:T(8,128)(2,1)} custom-call(bf16[512,256]{1,0:T(8,128)(2,1)S(1)} %attend_rest.1.own_ref, bf16[512,256]{1,0:T(8,128)(2,1)S(1)} %collective-permute-done.1.peer_ref, bf16[256,2048]{1,0:T(8,128)(2,1)S(1)} %copy-done.1, bf16[256,2048]{1,0:T(8,128)(2,1)S(1)} %collective-permute-done.2.w_peer_ref, bf16[512,2048]{1,0:T(8,128)(2,1)S(1)} %copy-done), custom_call_target="tpu_custom_call" | custom-call | flops 1073741824 | bytes 8388608 | tf_op jit(solution)/shard_map/finish/pallas_call | solution.py:447
  (1 shorter events, 0.0 us)
Async XLA Ops:
  0.0 33.7 %collective-permute-start = (bf16[1024,1024]{1,0:T(8,128)(2,1)}, bf16[1024,1024]{1,0:T(8,128)(2,1)}, u32[]{:S(2)}, u32[]{:S(2)}) collective-permute-start(bf16[1024,1024]{1,0:T(8,128)(2,1)} %own_ref.1), channel_id=1, source_target_pairs={{0,1},{1,0},{2,3},{3,2},{4,5},{5,4},{6,7},{7,6},{8,9},{9,8},{10,11... | collective-permute-start | bytes 6291464 | tf_op jit(solution)/shard_map/ppermute | solution.py:483
  2.7 19.7 %all-to-all-start = ((s32[64,2,16]{2,1,0:T(2,128)}), s32[64,2,16]{2,1,0:T(2,128)S(1)}, u32[]{:S(2)}, u32[]{:S(2)}) async-start(s32[64,2,16]{2,1,0:T(2,128)} %broadcast_in_dim.3), calls=%async_computation | async-start | bytes 131072 | tf_op jit(solution)/shard_map/all_to_all | solution.py:482
  25.3 61.7 %all-to-all-start.1 = ((bf16[64,64,512]{2,1,0:T(8,128)(2,1)}), bf16[64,64,512]{2,1,0:T(8,128)(2,1)}, u32[]{:S(2)}, u32[]{:S(2)}) async-start(bf16[64,64,512]{2,1,0:T(8,128)(2,1)} %fill_slots.1), calls=%async_computation.1 | async-start | bytes 8388608 | tf_op jit(solution)/shard_map/all_to_all | solution.py:495
  32.8 58.9 %collective-permute-start.5 = (bf16[768,2048]{1,0:T(8,128)(2,1)}, bf16[768,2048]{1,0:T(8,128)(2,1)}, u32[]{:S(2)}, u32[]{:S(2)}) collective-permute-start(bf16[768,2048]{1,0:T(8,128)(2,1)} %w_own_hbm.1), channel_id=1, source_target_pairs={{0,1},{1,0},{2,3},{3,2},{4,5},{5,4},{6,7},{7,6},{8,9},{9,8},{10,11... | collective-permute-start | bytes 9437192 | tf_op jit(solution)/shard_map/ppermute | solution.py:484
  58.6 6.0 %copy-start.1 = (bf16[256,2048]{1,0:T(8,128)(2,1)S(1)}, bf16[256,2048]{1,0:T(8,128)(2,1)}, u32[]{:S(2)}) copy-start(bf16[256,2048]{1,0:T(8,128)(2,1)} %w_own_ref.1) | copy-start | bytes 3145732
  58.6 6.4 %copy-start.6 = (s32[16,2]{0,1:T(2,128)S(1)}, s32[16,2]{0,1:T(2,128)}, u32[]{:S(2)}) copy-start(s32[16,2]{0,1:T(2,128)} %param.18) | copy-start | bytes 388
  58.6 2.2 %collective-permute-start.3 = (f32[1024,2]{1,0:T(8,128)}, f32[1024,2]{1,0:T(8,128)S(1)}, u32[]{:S(2)}, u32[]{:S(2)}) collective-permute-start(f32[1024,2]{1,0:T(8,128)} %get-tuple-element.18.refs_1_), channel_id=1, source_target_pairs={{0,1},{1,0},{2,3},{3,2},{4,5},{5,4},{6,7},{7,6},{8,9},{9,8},{10,11... | collective-permute-start | bytes 24584 | tf_op jit(solution)/shard_map/ppermute | solution.py:508
  60.8 0.8 copy-start.5
  64.2 22.7 %copy-start.3 = (bf16[1024,256]{1,0:T(8,128)(2,1)S(1)}, bf16[1024,256]{1,0:T(8,128)(2,1)}, u32[]{:S(2)}) copy-start(bf16[1024,256]{1,0:T(8,128)(2,1)} %get-tuple-element.14.q_ref) | copy-start | bytes 1572868
  64.2 22.7 %copy-start.4 = (bf16[256]{0:T(256)(128)(2,1)S(1)}, bf16[256]{0:T(256)(128)(2,1)}, u32[]{:S(2)}) copy-start(bf16[256]{0:T(256)(128)(2,1)} %param.31) | copy-start | bytes 1540
  64.3 27.5 %collective-permute-start.4 = (bf16[512,768]{1,0:T(8,128)(2,1)}, bf16[512,768]{1,0:T(8,128)(2,1)}, u32[]{:S(2)}, u32[]{:S(2)}) collective-permute-start(bf16[512,768]{1,0:T(8,128)(2,1)} %channel_swish.3), channel_id=1, source_target_pairs={{0,1},{1,0},{2,3},{3,2},{4,5},{5,4},{6,7},{7,6},{8,9},{9,8},{10,11... | collective-permute-start | bytes 2359304 | tf_op jit(solution)/shard_map/ppermute | solution.py:510
  64.5 36.0 %collective-permute-start.2 = (bf16[256,2048]{1,0:T(8,128)(2,1)S(1)}, bf16[256,2048]{1,0:T(8,128)(2,1)S(1)}, u32[]{:S(2)}, u32[]{:S(2)}) collective-permute-start(bf16[256,2048]{1,0:T(8,128)(2,1)S(1)} %copy-done.1), channel_id=1, source_target_pairs={{0,1},{1,0},{2,3},{3,2},{4,5},{5,4},{6,7},{7,6},{8,9},{9,8},{10,11... | collective-permute-start | bytes 3145736 | tf_op jit(solution)/shard_map/ppermute | solution.py:485
  67.8 24.0 %copy-start.2 = (bf16[512,768]{1,0:T(8,128)(2,1)S(1)}, bf16[512,768]{1,0:T(8,128)(2,1)}, u32[]{:S(2)}) copy-start(bf16[512,768]{1,0:T(8,128)(2,1)} %channel_swish.2.own_ref) | copy-start | bytes 2359300
  89.9 10.7 %collective-permute-start.1 = (bf16[512,256]{1,0:T(8,128)(2,1)S(1)}, bf16[512,256]{1,0:T(8,128)(2,1)S(1)}, u32[]{:S(2)}, u32[]{:S(2)}) collective-permute-start(bf16[512,256]{1,0:T(8,128)(2,1)S(1)} %get-tuple-element.17), channel_id=1, source_target_pairs={{0,1},{1,0},{2,3},{3,2},{4,5},{5,4},{6,7},{7,6},{8,9},{9,8},{10,11... | collective-permute-start | bytes 786440 | tf_op jit(solution)/shard_map/ppermute | solution.py:517
  100.6 1.6 %copy-start = (bf16[512,2048]{1,0:T(8,128)(2,1)S(1)}, bf16[512,2048]{1,0:T(8,128)(2,1)}, u32[]{:S(2)}) copy-start(bf16[512,2048]{1,0:T(8,128)(2,1)} %conv_product.1.conv_ref) | copy-start | bytes 6291460
where the time goes:
time: 105 us
  Pallas kernels  52.8 us (50%)
  waiting for transfers between devices  23.8 us (23%)
  starting transfers between devices  23.7 us (23%)
  local copies, waits for them, and re-layouts  3.92 us (4%)
    pallas_call x1, Pallas kernels, token_branch(): pl.pallas_call(token_kernel, out_shape=(jax.ShapeDtypeStruct((n, C_DEV),...  24.8 us
    all_to_all x1, waiting for transfers between devices, body(): received = lax.all_to_all(sent, 'st', 0, 0, tiled=True)  19.2 us
    all_to_all x1, starting transfers between devices, body(): lax.all_to_all(jnp.broadcast_to(passage_ids.T, (owner_count, *passage_ids...  11.2 us
    pallas_call x1, Pallas kernels, conv_product(): pl.pallas_call(pair_kernel, out_shape=pltpu.HBM((n, D), BF16), in_specs=[...  7.84 us
    all_to_all x1, starting transfers between devices, body(): received = lax.all_to_all(sent, 'st', 0, 0, tiled=True)  7.51 us
    pallas_call x1, Pallas kernels, project_store(): pl.pallas_call(kv_kernel, out_shape=pltpu.VMEM((n, 2 * MEM_DEV), BF16), i...  5.87 us
    pallas_call x2, Pallas kernels, channel_swish(): pl.pallas_call(lambda half_ref, *refs: swish_kernel(*refs), out_shape=jax...  5.33 us
    pallas_call x1, Pallas kernels, attend_first(): pl.pallas_call(attend_kernel, out_shape=(pltpu.VMEM((n, MEM_DEV), BF16),...  2.88 us
  transfers between devices with their start and end apart: 8, of which 3 were waited for; matrix products, arithmetic and copies ran while one was open for 1% of the time, Pallas kernels for 48%

commit v1 on v0

--- a/solution.py
+++ b/solution.py
@@ -21,6 +21,7 @@
 LAYER_EPS = 1e-05
 
 KV_TILE = 512
+COPY_ROWS = 256
 TOK_TILE = 256
 OUT_TILE = 256
 OUT_COLS = 512
@@ -72,12 +73,16 @@
 ):
     chunks = rows_hbm.shape[0] // KV_TILE
     span = lambda c: pl.ds(c * KV_TILE, KV_TILE)
-    row_copies = [pltpu.make_async_copy(rows_hbm.at[span(c)], rows_ref.at[span(c)], r_sem.at[c]) for c in range(chunks)]
+    pieces = KV_TILE // COPY_ROWS
+    part = lambda p: pl.ds(p * COPY_ROWS, COPY_ROWS)
+    row_copies = [
+        pltpu.make_async_copy(rows_hbm.at[part(p)], rows_ref.at[part(p)], r_sem.at[p]) for p in range(chunks * pieces)
+    ]
     wk_copy = pltpu.make_async_copy(wk_hbm, w_ref.at[:, :MEM_DEV], w_sem.at[0])
     wv_copy = pltpu.make_async_copy(wv_hbm, w_ref.at[:, MEM_DEV:], w_sem.at[1])
     gain_copy = pltpu.make_async_copy(gain_hbm, gain_ref, w_sem.at[2])
     kg_copy = pltpu.make_async_copy(kg_hbm, kg_ref, w_sem.at[3])
-    for c in [gain_copy, kg_copy, row_copies[0], wk_copy, wv_copy, *row_copies[1:]]:
+    for c in [gain_copy, kg_copy, *row_copies[:pieces], wk_copy, wv_copy, *row_copies[pieces:]]:
         c.start()
     gain_copy.wait()
     kg_copy.wait()
@@ -86,17 +91,17 @@
     held = (even, odd)
 
     def normalise(c):
-        for r in range(0, KV_TILE, NORM_ROWS):
-            rows = rows_ref[c * KV_TILE + r : c * KV_TILE + r + NORM_ROWS, :]
-            held[c % 2][r : r + NORM_ROWS, :] = row_norm(rows, gain)
-
-    row_copies[0].wait()
+        for p in range(pieces):
+            row_copies[c * pieces + p].wait()
+            for r in range(p * COPY_ROWS, (p + 1) * COPY_ROWS, NORM_ROWS):
+                rows = rows_ref[c * KV_TILE + r : c * KV_TILE + r + NORM_ROWS, :]
+                held[c % 2][r : r + NORM_ROWS, :] = row_norm(rows, gain)
+
     normalise(0)
     wk_copy.wait()
     wv_copy.wait()
     for c in range(chunks):
         if c + 1 < chunks:
-            row_copies[c + 1].wait()
             normalise(c + 1)
         both = matmul(held[c % 2][...], w_ref[...])
         out_ref[span(c), :MEM_DEV] = head_norm(both[:, :MEM_DEV], key_gain).astype(BF16)
@@ -138,7 +143,7 @@
             pltpu.VMEM((MEM_DEV // LANES, LANES), BF16),
             pltpu.VMEM((KV_TILE, D), BF16),
             pltpu.VMEM((KV_TILE, D), BF16),
-            pltpu.SemaphoreType.DMA((n // KV_TILE,)),
+            pltpu.SemaphoreType.DMA((n // COPY_ROWS,)),
             pltpu.SemaphoreType.DMA((4,)),
         ],
         compiler_params=grant(24),

time: 105 us -> 105 us (level)
  no operation moved by 1% of the time
where the time goes in v1:
time: 105 us; the launch traced here: 104 us
  Pallas kernels  52.7 us (50%)
  waiting for transfers between devices  23.9 us (23%)
  starting transfers between devices  23.6 us (22%)
  local copies, waits for them, and re-layouts  3.92 us (4%)
    pallas_call x1, Pallas kernels, token_branch(): pl.pallas_call(token_kernel, out_shape=(jax.ShapeDtypeStruct((n, C_DEV),...  24.8 us
    all_to_all x1, waiting for transfers between devices, body(): received = lax.all_to_all(sent, 'st', 0, 0, tiled=True)  19.2 us
    all_to_all x1, starting transfers between devices, body(): lax.all_to_all(jnp.broadcast_to(passage_ids.T, (owner_count, *passage_ids...  11.2 us
    pallas_call x1, Pallas kernels, conv_product(): pl.pallas_call(pair_kernel, out_shape=pltpu.HBM((n, D), BF16), in_specs=[...  7.84 us
    all_to_all x1, starting transfers between devices, body(): received = lax.all_to_all(sent, 'st', 0, 0, tiled=True)  7.4 us
    pallas_call x1, Pallas kernels, project_store(): pl.pallas_call(kv_kernel, out_shape=pltpu.VMEM((n, 2 * MEM_DEV), BF16), i...  5.76 us
    pallas_call x2, Pallas kernels, channel_swish(): pl.pallas_call(lambda half_ref, *refs: swish_kernel(*refs), out_shape=jax...  5.33 us
    pallas_call x1, Pallas kernels, attend_first(): pl.pallas_call(attend_kernel, out_shape=(pltpu.VMEM((n, MEM_DEV), BF16),...  2.88 us
  transfers between devices with their start and end apart: 8, of which 3 were waited for; matrix products, arithmetic and copies ran while one was open for 1% of the time, Pallas kernels for 48%

profile of v1, /device:TPU:1, one launch (start us, length us, event | category | flops | bytes accessed | tf_op | source)
XLA Modules:
  0.0 104.4 jit_solution(15179927593328978454)
XLA Ops:
  0.0 1.4 %collective-permute-start = (bf16[1024,1024]{1,0:T(8,128)(2,1)}, bf16[1024,1024]{1,0:T(8,128)(2,1)}, u32[]{:S(2)}, u32[]{:S(2)}) collective-permute-start(bf16[1024,1024]{1,0:T(8,128)(2,1)} %own_ref.1), channel_id=1, source_target_pairs={{0,1},{1,0},{2,3},{3,2},{4,5},{5,4},{6,7},{7,6},{8,9},{9,8},{10,11... | collective-permute-start | bytes 6291464 | tf_op jit(solution)/shard_map/ppermute | solution.py:488
  1.4 1.3 %broadcast_in_dim.3 = s32[64,2,16]{2,1,0:T(2,128)} broadcast(s32[2,16]{1,0:T(2,128)} %bitcast.15), dimensions={1,2} | broadcast | bytes 8320 | tf_op jit(solution)/shard_map/broadcast_in_dim | solution.py:487
  2.7 11.2 %all-to-all-start = ((s32[64,2,16]{2,1,0:T(2,128)}), s32[64,2,16]{2,1,0:T(2,128)S(1)}, u32[]{:S(2)}, u32[]{:S(2)}) async-start(s32[64,2,16]{2,1,0:T(2,128)} %broadcast_in_dim.3), calls=%async_computation | async-start | bytes 131072 | tf_op jit(solution)/shard_map/all_to_all | solution.py:487
  14.0 5.8 %project_store.1 = bf16[1024,512]{1,0:T(8,128)(2,1)S(1)} custom-call(bf16[1024,2048]{1,0:T(8,128)(2,1)} %bitcast.16, bf16[16,128]{1,0:T(8,128)(2,1)} %bitcast.17, bf16[2048,256]{1,0:T(8,128)(2,1)} %wk_hbm.1, bf16[2048,256]{1,0:T(8,128)(2,1)} %wv_hbm.1, bf16[2,128]{1,0:T(2,128)(2,1)} %bitcast.19), custom_call_target="tpu_custom_call" | custom-call | flops 2147483648 | bytes 8388608 | tf_op jit(solution)/shard_map/project_store/pallas_call | solution.py:134
  19.7 2.7 %all-to-all-done.ids_ref = s32[64,2,16]{2,1,0:T(2,128)S(1)} async-done(((s32[64,2,16]{2,1,0:T(2,128)}), s32[64,2,16]{2,1,0:T(2,128)S(1)}, u32[]{:S(2)}, u32[]{:S(2)}) %all-to-all-start) | async-done | bytes 8224 | tf_op jit(solution)/shard_map/all_to_all | solution.py:487
  22.4 2.9 %fill_slots.1 = bf16[64,64,512]{2,1,0:T(8,128)(2,1)} custom-call(s32[64,2,16]{2,1,0:T(2,128)S(1)} %all-to-all-done.ids_ref, bf16[16,64,512]{2,1,0:T(8,128)(2,1)S(1)} %bitcast.10), custom_call_target="tpu_custom_call" | custom-call | tf_op jit(solution)/shard_map/fill_slots/pallas_call | solution.py:171
  25.3 7.4 %all-to-all-start.1 = ((bf16[64,64,512]{2,1,0:T(8,128)(2,1)}), bf16[64,64,512]{2,1,0:T(8,128)(2,1)}, u32[]{:S(2)}, u32[]{:S(2)}) async-start(bf16[64,64,512]{2,1,0:T(8,128)(2,1)} %fill_slots.1), calls=%async_computation.1 | async-start | bytes 8388608 | tf_op jit(solution)/shard_map/all_to_all | solution.py:500
  32.7 0.9 collective-permute-start.5
  33.6 0.0 collective-permute-done.peer_ref
  33.6 24.8 %token_branch.1 = (f32[1024,768]{1,0:T(8,128)}, f32[1024,2]{1,0:T(8,128)}, bf16[1024,256]{1,0:T(8,128)(2,1)}) custom-call(s32[1]{0:T(128)} %bitcast.tp_ref.half_ref, bf16[1024,1024]{1,0:T(8,128)(2,1)} %own_ref.1, bf16[1024,1024]{1,0:T(8,128)(2,1)} %collective-permute-done.peer_ref, bf16[2,8,128]{2,1,0:T(8,128)(2,1)} %bitcast.18, bf16[2048,768]{1,0:T(8,128)(2,1)} %wv_ref.1, ...), custom_call_target="tpu_custom_call" | custom-call | flops 32212254720 | bytes 16777216 | tf_op jit(solution)/shard_map/token_branch/pallas_call | solution.py:244
  58.4 0.0 copy-start.1
  58.4 0.0 copy-start.6
  58.4 0.3 collective-permute-start.3
  58.8 2.1 %collective-permute-done.3.refs_2_ = f32[1024,2]{1,0:T(8,128)S(1)} collective-permute-done((f32[1024,2]{1,0:T(8,128)}, f32[1024,2]{1,0:T(8,128)S(1)}, u32[]{:S(2)}, u32[]{:S(2)}) %collective-permute-start.3) | collective-permute-done | bytes 8224 | tf_op jit(solution)/shard_map/ppermute | solution.py:513
  60.8 0.0 copy-start.5
  60.8 0.8 copy-done.5
  61.6 2.7 %channel_swish.3 = bf16[512,768]{1,0:T(8,128)(2,1)} custom-call(s32[1]{0:T(128)S(6)} %sub.3.half_ref, f32[1024,768]{1,0:T(8,128)} %get-tuple-element.12.refs_0_, f32[1024,2]{1,0:T(8,128)} %get-tuple-element.18.refs_1_, f32[1024,2]{1,0:T(8,128)} %copy-done.5, bf16[6,128]{1,0:T(8,128)(2,1)} %bitcast.13), custom_call_target="tpu_custom_call" | custom-call | flops 805306368 | bytes 4194304 | tf_op jit(solution)/shard_map/channel_swish/pallas_call | solution.py:289
  64.3 0.0 copy-start.3
  64.3 0.0 copy-start.4
  64.3 0.1 collective-permute-start.4
  64.5 0.0 copy-done.1
  64.5 0.4 collective-permute-start.2
  64.8 0.0 copy-done.6
  64.8 0.1 copy.19
  64.9 0.1 shift_right_arithmetic.10.owner_ref
  65.0 2.7 %channel_swish.2.own_ref = bf16[512,768]{1,0:T(8,128)(2,1)} custom-call(s32[1]{0:T(128)} %bitcast.tp_ref.half_ref, f32[1024,768]{1,0:T(8,128)} %get-tuple-element.12.refs_0_, f32[1024,2]{1,0:T(8,128)} %get-tuple-element.18.refs_1_, f32[1024,2]{1,0:T(8,128)} %copy-done.5, bf16[6,128]{1,0:T(8,128)(2,1)} %bitcast.14), custom_call_target="tpu_custom_call" | custom-call | flops 805306368 | bytes 4194304 | tf_op jit(solution)/shard_map/channel_swish/pallas_call | solution.py:289
  67.7 0.0 copy-start.2
  67.7 19.2 %all-to-all-done.1.recv_hbm = bf16[64,64,512]{2,1,0:T(8,128)(2,1)} async-done(((bf16[64,64,512]{2,1,0:T(8,128)(2,1)}), bf16[64,64,512]{2,1,0:T(8,128)(2,1)}, u32[]{:S(2)}, u32[]{:S(2)}) %all-to-all-start.1) | async-done | bytes 4194336 | tf_op jit(solution)/shard_map/all_to_all | solution.py:500
  86.9 0.0 copy-done.3
  86.9 0.0 copy-done.4
  86.9 2.9 %attend_first.1 = (bf16[512,256]{1,0:T(8,128)(2,1)S(1)}, bf16[16,64,512]{2,1,0:T(8,128)(2,1)S(1)}, bf16[512,256]{1,0:T(8,128)(2,1)S(1)}) custom-call(s32[1,32]{1,0:T(1,128)S(1)} %shift_right_arithmetic.10.owner_ref, bf16[64,64,512]{2,1,0:T(8,128)(2,1)} %all-to-all-done.1.recv_hbm, bf16[1024,256]{1,0:T(8,128)(2,1)S(1)} %copy-done.3, bf16[2,128]{1,0:T(2,128)(2,1)S(1)} %bitcast.11), custom_call_target="tpu_custom_call" | custom-call | flops 268435456 | bytes 2097152 | tf_op jit(solution)/shard_map/attend_first/pallas_call | solution.py:400
  89.8 1.8 %collective-permute-start.1 = (bf16[512,256]{1,0:T(8,128)(2,1)S(1)}, bf16[512,256]{1,0:T(8,128)(2,1)S(1)}, u32[]{:S(2)}, u32[]{:S(2)}) collective-permute-start(bf16[512,256]{1,0:T(8,128)(2,1)S(1)} %get-tuple-element.17), channel_id=1, source_target_pairs={{0,1},{1,0},{2,3},{3,2},{4,5},{5,4},{6,7},{7,6},{8,9},{9,8},{10,11... | collective-permute-start | bytes 786440 | tf_op jit(solution)/shard_map/ppermute | solution.py:522
  91.6 0.0 collective-permute-done.4.peer_ref
  91.6 0.0 collective-permute-done.5.w_peer_hbm
  91.6 0.0 copy-done.2
  91.6 7.8 %conv_product.1.conv_ref = bf16[512,2048]{1,0:T(8,128)(2,1)} custom-call(bf16[512,768]{1,0:T(8,128)(2,1)S(1)} %copy-done.2, bf16[512,768]{1,0:T(8,128)(2,1)} %collective-permute-done.4.peer_ref, bf16[768,2048]{1,0:T(8,128)(2,1)} %w_own_hbm.1, bf16[768,2048]{1,0:T(8,128)(2,1)} %collective-permute-done.5.w_peer_hbm), custom_call_target="tpu_custom_call" | custom-call | flops 3221225472 | bytes 12582912 | tf_op jit(solution)/shard_map/conv_product/pallas_call | solution.py:322
  99.4 1.0 attend_rest.1.own_ref
  100.4 0.0 collective-permute-done.2.w_peer_ref
  100.4 0.0 collective-permute-done.1.peer_ref
  100.4 0.0 copy-start
  100.4 1.6 %copy-done = bf16[512,2048]{1,0:T(8,128)(2,1)S(1)} copy-done((bf16[512,2048]{1,0:T(8,128)(2,1)S(1)}, bf16[512,2048]{1,0:T(8,128)(2,1)}, u32[]{:S(2)}) %copy-start) | copy-done | bytes 2097176
  102.0 2.2 %finish.1 = bf16[512,2048]{1,0:T(8,128)(2,1)} custom-call(bf16[512,256]{1,0:T(8,128)(2,1)S(1)} %attend_rest.1.own_ref, bf16[512,256]{1,0:T(8,128)(2,1)S(1)} %collective-permute-done.1.peer_ref, bf16[256,2048]{1,0:T(8,128)(2,1)S(1)} %copy-done.1, bf16[256,2048]{1,0:T(8,128)(2,1)S(1)} %collective-permute-done.2.w_peer_ref, bf16[512,2048]{1,0:T(8,128)(2,1)S(1)} %copy-done), custom_call_target="tpu_custom_call" | custom-call | flops 1073741824 | bytes 8388608 | tf_op jit(solution)/shard_map/finish/pallas_call | solution.py:452
  (1 shorter events, 0.0 us)
Async XLA Ops:
  0.0 33.6 %collective-permute-start = (bf16[1024,1024]{1,0:T(8,128)(2,1)}, bf16[1024,1024]{1,0:T(8,128)(2,1)}, u32[]{:S(2)}, u32[]{:S(2)}) collective-permute-start(bf16[1024,1024]{1,0:T(8,128)(2,1)} %own_ref.1), channel_id=1, source_target_pairs={{0,1},{1,0},{2,3},{3,2},{4,5},{5,4},{6,7},{7,6},{8,9},{9,8},{10,11... | collective-permute-start | bytes 6291464 | tf_op jit(solution)/shard_map/ppermute | solution.py:488
  2.7 19.7 %all-to-all-start = ((s32[64,2,16]{2,1,0:T(2,128)}), s32[64,2,16]{2,1,0:T(2,128)S(1)}, u32[]{:S(2)}, u32[]{:S(2)}) async-start(s32[64,2,16]{2,1,0:T(2,128)} %broadcast_in_dim.3), calls=%async_computation | async-start | bytes 131072 | tf_op jit(solution)/shard_map/all_to_all | solution.py:487
  25.3 61.6 %all-to-all-start.1 = ((bf16[64,64,512]{2,1,0:T(8,128)(2,1)}), bf16[64,64,512]{2,1,0:T(8,128)(2,1)}, u32[]{:S(2)}, u32[]{:S(2)}) async-start(bf16[64,64,512]{2,1,0:T(8,128)(2,1)} %fill_slots.1), calls=%async_computation.1 | async-start | bytes 8388608 | tf_op jit(solution)/shard_map/all_to_all | solution.py:500
  32.7 58.9 %collective-permute-start.5 = (bf16[768,2048]{1,0:T(8,128)(2,1)}, bf16[768,2048]{1,0:T(8,128)(2,1)}, u32[]{:S(2)}, u32[]{:S(2)}) collective-permute-start(bf16[768,2048]{1,0:T(8,128)(2,1)} %w_own_hbm.1), channel_id=1, source_target_pairs={{0,1},{1,0},{2,3},{3,2},{4,5},{5,4},{6,7},{7,6},{8,9},{9,8},{10,11... | collective-permute-start | bytes 9437192 | tf_op jit(solution)/shard_map/ppermute | solution.py:489
  58.4 6.0 %copy-start.1 = (bf16[256,2048]{1,0:T(8,128)(2,1)S(1)}, bf16[256,2048]{1,0:T(8,128)(2,1)}, u32[]{:S(2)}) copy-start(bf16[256,2048]{1,0:T(8,128)(2,1)} %w_own_ref.1) | copy-start | bytes 3145732
  58.4 6.4 %copy-start.6 = (s32[16,2]{0,1:T(2,128)S(1)}, s32[16,2]{0,1:T(2,128)}, u32[]{:S(2)}) copy-start(s32[16,2]{0,1:T(2,128)} %param.18) | copy-start | bytes 388
  58.4 2.4 %collective-permute-start.3 = (f32[1024,2]{1,0:T(8,128)}, f32[1024,2]{1,0:T(8,128)S(1)}, u32[]{:S(2)}, u32[]{:S(2)}) collective-permute-start(f32[1024,2]{1,0:T(8,128)} %get-tuple-element.18.refs_1_), channel_id=1, source_target_pairs={{0,1},{1,0},{2,3},{3,2},{4,5},{5,4},{6,7},{7,6},{8,9},{9,8},{10,11... | collective-permute-start | bytes 24584 | tf_op jit(solution)/shard_map/ppermute | solution.py:513
  60.8 0.8 copy-start.5
  64.3 22.6 %copy-start.3 = (bf16[1024,256]{1,0:T(8,128)(2,1)S(1)}, bf16[1024,256]{1,0:T(8,128)(2,1)}, u32[]{:S(2)}) copy-start(bf16[1024,256]{1,0:T(8,128)(2,1)} %get-tuple-element.14.q_ref) | copy-start | bytes 1572868
  64.3 22.6 %copy-start.4 = (bf16[256]{0:T(256)(128)(2,1)S(1)}, bf16[256]{0:T(256)(128)(2,1)}, u32[]{:S(2)}) copy-start(bf16[256]{0:T(256)(128)(2,1)} %param.31) | copy-start | bytes 1540
  64.3 27.3 %collective-permute-start.4 = (bf16[512,768]{1,0:T(8,128)(2,1)}, bf16[512,768]{1,0:T(8,128)(2,1)}, u32[]{:S(2)}, u32[]{:S(2)}) collective-permute-start(bf16[512,768]{1,0:T(8,128)(2,1)} %channel_swish.3), channel_id=1, source_target_pairs={{0,1},{1,0},{2,3},{3,2},{4,5},{5,4},{6,7},{7,6},{8,9},{9,8},{10,11... | collective-permute-start | bytes 2359304 | tf_op jit(solution)/shard_map/ppermute | solution.py:515
  64.5 35.9 %collective-permute-start.2 = (bf16[256,2048]{1,0:T(8,128)(2,1)S(1)}, bf16[256,2048]{1,0:T(8,128)(2,1)S(1)}, u32[]{:S(2)}, u32[]{:S(2)}) collective-permute-start(bf16[256,2048]{1,0:T(8,128)(2,1)S(1)} %copy-done.1), channel_id=1, source_target_pairs={{0,1},{1,0},{2,3},{3,2},{4,5},{5,4},{6,7},{7,6},{8,9},{9,8},{10,11... | collective-permute-start | bytes 3145736 | tf_op jit(solution)/shard_map/ppermute | solution.py:490
  67.7 23.9 %copy-start.2 = (bf16[512,768]{1,0:T(8,128)(2,1)S(1)}, bf16[512,768]{1,0:T(8,128)(2,1)}, u32[]{:S(2)}) copy-start(bf16[512,768]{1,0:T(8,128)(2,1)} %channel_swish.2.own_ref) | copy-start | bytes 2359300
  89.8 10.7 %collective-permute-start.1 = (bf16[512,256]{1,0:T(8,128)(2,1)S(1)}, bf16[512,256]{1,0:T(8,128)(2,1)S(1)}, u32[]{:S(2)}, u32[]{:S(2)}) collective-permute-start(bf16[512,256]{1,0:T(8,128)(2,1)S(1)} %get-tuple-element.17), channel_id=1, source_target_pairs={{0,1},{1,0},{2,3},{3,2},{4,5},{5,4},{6,7},{7,6},{8,9},{9,8},{10,11... | collective-permute-start | bytes 786440 | tf_op jit(solution)/shard_map/ppermute | solution.py:522
  100.4 1.6 %copy-start = (bf16[512,2048]{1,0:T(8,128)(2,1)S(1)}, bf16[512,2048]{1,0:T(8,128)(2,1)}, u32[]{:S(2)}) copy-start(bf16[512,2048]{1,0:T(8,128)(2,1)} %conv_product.1.conv_ref) | copy-start | bytes 6291460
